TPU v7x, 32 devices: a whole 2x2x4 slice. The times are simulated.
32 devices in a mesh: kv: 8 (over z, y), tp: 4 (over x, core).
Axes of the slice: x: 2, y: 2, z: 4, core: 2. Of those that a mesh axis runs over, the one named last changes fastest.
Arguments:
- tokens: bfloat16 [32, 4096], P(None, 'kv'), may hold values from -40 to 40, as said below
- norm_gain: float32 [4096], P('kv'), may hold values from 0.1 to 1.9
- w_query: bfloat16 [4096, 2048], P('kv', 'tp'), may hold values from -0.09375 to 0.09375
- w_key: bfloat16 [4096, 512], P('kv', 'tp'), may hold values from -0.09375 to 0.09375
- w_value: bfloat16 [4096, 512], P('kv', 'tp'), may hold values from -0.09375 to 0.09375
- forget_weight: bfloat16 [4096, 32], replicated, may hold values from -0.09375 to 0.09375
- forget_bias: float32 [32], P('tp'), may hold values from -1 to 3
- kv_cache: bfloat16 [32, 10240, 8, 128], P(None, 'kv', 'tp'), may hold values from -6 to 6
- cum_gates: float32 [32, 32, 10240], P(None, 'tp', 'kv'), may hold values from -10500 to 0, as said below
- lengths: int32 [32], replicated, may hold values from 1 to 10240, as said below
- w_out: bfloat16 [2048, 4096], P('tp', 'kv'), may hold values from -0.25 to 0.25
Outputs:
- mixed: bfloat16 [32, 4096], P(None, 'kv')
- log_weight: float32 [32, 32], P(None, 'tp')
Inputs may be any that keep to these rules, and one draw needn't show every extreme that they name: Columns of tokens come in 16 groups of equal width. `cum_gates`: each row does not rise along the positions. `lengths`: some sequence has all 10240 positions cached.
All inputs are finite; a program needn't handle non-finite values.
Results may differ from a plain program's by a relative error of at most 0.0307.
Values may be sent and summed in bfloat16 or wider, within the bound.
A program may use at most 128 MiB of HBM per device.

v0:
```python
import jax
import jax.numpy as jnp
from jax import lax
from jax.sharding import PartitionSpec as P

norm_eps = 1e-05
masked_floor = -1e30


def finish_rows(row_squares, sum_query, sum_keyval, sum_gate, forget_bias, model_width):
    row_scale = lax.rsqrt(row_squares / model_width + norm_eps)[:, None]
    query = (row_scale * sum_query).astype(jnp.bfloat16)
    keyval = (row_scale * sum_keyval).astype(jnp.bfloat16)
    log_gate = jax.nn.log_sigmoid(row_scale * sum_gate + forget_bias)
    return (query, keyval, log_gate)


def shards(
    tokens,
    norm_gain,
    w_query,
    w_key,
    w_value,
    forget_weight,
    forget_bias,
    kv_cache,
    cum_gates,
    lengths,
    w_out,
):
    rows_count, col_count = tokens.shape
    span_len = kv_cache.shape[1]
    kv_local = kv_cache.shape[2]
    head_size = kv_cache.shape[3] // 2
    heads_local = cum_gates.shape[1]
    group_size = heads_local // kv_local
    model_width = col_count * lax.axis_size("kv")
    tokens_f = tokens.astype(jnp.float32)
    squares = jnp.sum(tokens_f * tokens_f, axis=1)
    normalized_input = (tokens_f * norm_gain).astype(jnp.bfloat16)
    gate_cols = lax.dynamic_slice(
        forget_weight,
        (lax.axis_index("kv") * col_count, lax.axis_index("tp") * heads_local),
        (col_count, heads_local),
    )
    part_query = jnp.dot(normalized_input, w_query, preferred_element_type=jnp.float32)
    part_keyval = jnp.concatenate(
        [
            jnp.dot(normalized_input, w_key, preferred_element_type=jnp.float32),
            jnp.dot(normalized_input, w_value, preferred_element_type=jnp.float32),
        ],
        axis=1,
    )
    part_gate = jnp.dot(normalized_input, gate_cols, preferred_element_type=jnp.float32)
    total_sq, sum_query, sum_keyval, sum_gate = (
        lax.psum(squares.astype(jnp.bfloat16), "kv").astype(jnp.float32),
        lax.psum(part_query.astype(jnp.bfloat16), "kv").astype(jnp.float32),
        lax.psum(part_keyval.astype(jnp.bfloat16), "kv").astype(jnp.float32),
        lax.psum(part_gate.astype(jnp.bfloat16), "kv").astype(jnp.float32),
    )
    query, keyval, log_gate = finish_rows(
        total_sq, sum_query, sum_keyval, sum_gate, forget_bias, model_width
    )
    inv_root = head_size ** (-0.5)
    query_head_rows = query.reshape(rows_count, kv_local, group_size, head_size)
    cached_keys = kv_cache[:, :, :, :head_size]
    cached_vals = kv_cache[:, :, :, head_size:]
    scores = (
        jnp.einsum(
            "bkgd,blkd->bkgl", query_head_rows, cached_keys, preferred_element_type=jnp.float32
        )
        * inv_root
    )
    biased = scores - cum_gates.reshape(rows_count, kv_local, group_size, span_len)
    first_pos = lax.axis_index("kv") * span_len
    positions = first_pos + lax.iota(jnp.int32, span_len)
    in_range = positions[None, :] < lengths[:, None]
    last_pos = lengths - 1
    holds_last = (last_pos >= first_pos) & (last_pos < first_pos + span_len)
    last_index = jnp.clip(last_pos - first_pos, 0, span_len - 1)
    last_cum = jnp.take_along_axis(
        cum_gates, jnp.broadcast_to(last_index[:, None, None], (rows_count, heads_local, 1)), axis=2
    )[:, :, 0]
    cum_query = last_cum + log_gate
    fresh_key_row = keyval[:, : kv_local * head_size].reshape(rows_count, kv_local, head_size)
    value_new = keyval[:, kv_local * head_size :].reshape(rows_count, kv_local, head_size)
    new_biased = (
        jnp.einsum(
            "pnof,pnf->pno", query_head_rows, fresh_key_row, preferred_element_type=jnp.float32
        )
        * inv_root
    )
    new_biased = new_biased - cum_query.reshape(rows_count, kv_local, group_size)
    range_mask = in_range[:, None, None, :]
    owner_mask = holds_last[:, None, None]
    peak_local = jnp.max(jnp.where(range_mask, biased, masked_floor), axis=-1)
    peak_local = jnp.where(owner_mask, jnp.maximum(peak_local, new_biased), peak_local)
    weights = jnp.where(range_mask, jnp.exp(biased - peak_local[..., None]), 0.0)
    new_weight = jnp.where(owner_mask, jnp.exp(new_biased - peak_local), 0.0)
    weight_sum = jnp.sum(weights, axis=-1) + new_weight
    weighted = jnp.einsum(
        "bkgl,blkd->bkgd",
        weights.astype(jnp.bfloat16),
        cached_vals,
        preferred_element_type=jnp.float32,
    )
    weighted = (
        weighted
        + new_weight.astype(jnp.bfloat16).astype(jnp.float32)[..., None]
        * value_new.astype(jnp.float32)[:, :, None, :]
    )
    anchor = jnp.where(holds_last[:, None], cum_query, 0.0).reshape(
        rows_count, kv_local, group_size
    )
    peak = lax.pmax(peak_local, "kv")
    rescale_factor = jnp.exp(peak_local - peak)
    weight_sum, weighted, anchor = lax.psum(
        (weight_sum * rescale_factor, weighted * rescale_factor[..., None], anchor), "kv"
    )
    attended = (
        (weighted / weight_sum[..., None])
        .astype(jnp.bfloat16)
        .reshape(rows_count, heads_local * head_size)
    )
    log_weight = (peak + jnp.log(weight_sum) + anchor).reshape(rows_count, heads_local)
    part_out = jnp.dot(attended, w_out, preferred_element_type=jnp.float32)
    mixed = lax.psum(part_out.astype(jnp.bfloat16), "tp")
    return (mixed, log_weight)


def solution(mesh):
    placed = (
        P(None, "kv"),
        P("kv"),
        P("kv", "tp"),
        P("kv", "tp"),
        P("kv", "tp"),
        P(),
        P("tp"),
        P(None, "kv", "tp", None),
        P(None, "tp", "kv"),
        P(),
        P("tp", "kv"),
    )
    return jax.shard_map(
        shards,
        mesh=mesh,
        in_specs=placed,
        out_specs=(P(None, "kv"), P(None, "tp")),
        check_vma=False,
    )
```

profile of v0, /device:TPU:0, one launch (start us, length us, event | category | flops | bytes accessed | tf_op | source)
XLA Modules:
  0.0 224.6 jit_solution(18268263765218162662)
XLA Ops:
  7.2 0.0 copy-start
  7.2 0.0 all-reduce.4.cloned.1.call-start
  7.2 0.0 copy-start.2
  7.3 41.6 %fusion.40 = (bf16[32,1280,2,64]{3,2,1,0:T(2,128)(2,1)}, bf16[32,1280,2,64]{3,2,1,0:T(2,128)(2,1)}) fusion(bf16[32,1280,2,128]{3,2,1,0:T(2,128)(2,1)} %param.18), kind=kLoop, calls=%fused_computation.64 | loop fusion | bytes 41943040 | tf_op jit(solution)/shard_map/slice | solution.py:66
  48.9 0.0 copy-start.5
  48.9 0.0 copy-start.6
  48.9 1.5 reshape.198
  50.4 0.1 fusion.22
  50.5 0.2 convolution_convert_fusion.1
  50.7 0.1 convolution_convert_fusion.2
  50.9 0.0 copy-done.6
  50.9 0.1 convolution_convert_fusion.3
  51.0 0.8 convolution_convert_fusion.4
  51.8 39.3 %all-reduce.1 = (bf16[32,512]{1,0:T(8,128)(2,1)S(1)}, bf16[32]{0:T(256)(128)(2,1)S(1)}, bf16[32,8]{0,1:T(8,128)(2,1)S(1)}, bf16[32,256]{1,0:T(8,128)(2,1)S(1)}) all-reduce(bf16[32,512]{1,0:T(8,128)(2,1)S(1)} %convolution_convert_fusion.1, bf16[32]{0:T(256)(128)(2,1)S(1)} %fusion.22, ...), channel_id=1, replica_groups=mesh['kv'=8,'tp'=4] {'kv'}, use_global_device_ids=true, to_apply=%region_2.0 | all-reduce | flops 24864 | bytes 99456 | tf_op jit(solution)/shard_map/psum | solution.py:57
  91.2 0.1 multiply_convert_fusion
  91.3 0.1 reshape.197
  91.4 0.1 broadcast_compare_fusion
  91.5 12.1 %select_reduce_fusion = (f32[32,2,4]{2,1,0:T(2,128)S(1)}, f32[32,2,4,1280]{3,2,1,0:T(4,128)S(1)}) fusion(pred[32,1280]{1,0:T(8,128)(4,1)S(1)} %broadcast_compare_fusion, f32[32,2,4,1280]{3,2,1,0:T(4,128)} %reshape.198, bf16[32,2,4,64]{3,2,1,0:T(4,128)(2,1)S(1)} %reshape.197, bf16[32,1280,2,64]{3,2,1,0:T(2,128)(2,1)} %get-tuple-element.15), kind=kOutput, calls=%fused_computation.8 | convolution fusion | flops 43253504 | bytes 13181952 | tf_op jit(solution)/shard_map/bkgd,blkd->bkgl/dot_general | solution.py:69
  103.6 0.1 copy.42
  103.8 0.1 copy.40
  103.9 0.1 reshape.207
  103.9 0.0 copy-start.9
  104.0 2.3 %gather_fusion = f32[256]{0:T(256)S(1)} fusion(f32[32,8,1280]{2,1,0:T(8,128)S(1)} %copy-done.2, s32[256]{0:T(256)S(1)} %reshape.207), kind=kCustom, calls=%fused_computation | custom fusion | bytes 5120 | tf_op jit(solution)/shard_map/jit(take_along_axis)/gather | solution.py:81
  106.2 0.1 gather.7
  106.3 0.1 copy.41
  106.4 0.1 multiply_convert_fusion.1
  106.5 0.1 reshape.218
  106.6 0.2 fusion.41
  106.8 0.1 copy.51
  106.9 0.1 broadcast_select_fusion
  107.0 0.1 copy.44
  107.1 17.1 %pmax.7 = f32[32,2,4]{0,2,1:T(4,128)S(1)} all-reduce(f32[32,2,4]{0,2,1:T(4,128)S(1)} %maximum_select_fusion), channel_id=1, replica_groups=mesh['kv'=8,'tp'=4] {'kv'}, use_global_device_ids=true, to_apply=%region_6.7 | all-reduce | flops 256 | bytes 2048 | tf_op jit(solution)/shard_map/pmax | solution.py:115
  124.2 0.8 fusion.16
  125.0 0.1 copy.48
  125.1 0.1 copy.47
  125.2 0.1 reshape.204
  125.3 0.1 copy.46
  125.4 0.0 copy-start.1
  125.4 10.7 %fusion.13 = f32[32,2,4,64]{3,2,1,0:T(4,128)} fusion(bf16[32,1280,2,64]{3,2,1,0:T(2,128)(2,1)} %get-tuple-element.16, f32[32,2,4,1280]{3,2,1,0:T(4,128)S(1)} %get-tuple-element.21, f32[32,2,4]{2,1,0:T(2,128)S(1)} %copy.44, pred[32,1280]{1,0:T(8,128)(4,1)S(1)} %broadcast_compare_fusion, f32[32,2,4]{2,1,0:T(2,128)S(1)} %copy.47, ...), kind=kOutput, calls=%fused_computation.10 | convolution fusion | flops 42975232 | bytes 11922432 | tf_op jit(solution)/shard_map/bkgl,blkd->bkgd/dot_general | solution.py:101
  136.2 0.0 all-reduce.4.cloned.1.call-update
  136.2 19.6 %all-reduce = (f32[32,2,4]{0,2,1:T(4,128)S(1)}, f32[32,2,4]{0,2,1:T(4,128)S(1)}) all-reduce(f32[32,2,4]{0,2,1:T(4,128)S(1)} %get-tuple-element.10, f32[32,2,4]{0,2,1:T(4,128)S(1)} %bitcast.31), channel_id=1, replica_groups=mesh['kv'=8,'tp'=4] {'kv'}, use_global_device_ids=true, to_apply=%region_9.10 | all-reduce | flops 512 | bytes 4096 | tf_op jit(solution)/shard_map/psum | solution.py:117
  155.8 0.6 add_add_fusion
  156.4 0.1 copy.49
  156.5 49.0 %all-reduce.4.cloned.1.call-done = f32[32,2,4,64]{3,2,1,0:T(4,128)} async-done(((f32[32,2,4,64]{3,2,1,0:T(4,128)}), f32[32,2,4,64]{3,2,1,0:T(4,128)}) %all-reduce.4.cloned.1.call-update) | async-done | bytes 65552 | tf_op jit(solution)/shard_map/psum | solution.py:117
  205.5 1.0 divide_convert_fusion
  206.5 0.1 reshape.201
  206.7 0.2 convolution_convert_fusion
  206.9 10.9 %psum.62 = bf16[32,512]{1,0:T(8,128)(2,1)} all-reduce(bf16[32,512]{1,0:T(8,128)(2,1)S(1)} %convolution_convert_fusion), channel_id=1, replica_groups=mesh['kv'=8,'tp'=4] {'tp'}, use_global_device_ids=true, to_apply=%region_10.11 | all-reduce | flops 16384 | bytes 65536 | tf_op jit(solution)/shard_map/psum | solution.py:127
  (26 shorter events, 0.1 us)
Async XLA Ops:
  7.2 43.3 %copy-start = (bf16[512,512]{1,0:T(8,128)(2,1)S(1)}, bf16[512,512]{1,0:T(8,128)(2,1)}, u32[]{:S(2)}) copy-start(bf16[512,512]{1,0:T(8,128)(2,1)} %param.13) | copy-start | bytes 1572868
  7.2 198.3 %all-reduce.4.cloned.1.call-start = ((), (), s32[]{:S(2)}) async-start(), calls=%async_computation | async-start | bytes 262144 | tf_op jit(solution)/shard_map/psum | solution.py:117
  7.2 41.6 %copy-start.2 = (f32[32,8,1280]{2,1,0:T(8,128)S(1)}, f32[32,8,1280]{2,1,0:T(8,128)}, u32[]{:S(2)}) copy-start(f32[32,8,1280]{2,1,0:T(8,128)} %param.19) | copy-start | bytes 3932164
  48.9 1.5 copy-start.3
  48.9 1.6 copy-start.7
  48.9 1.8 copy-start.5
  48.9 2.0 copy-start.6
  48.9 42.5 %copy-start.8 = (s32[32]{0:T(128)S(1)}, s32[32]{0:T(128)}, u32[]{:S(2)}) copy-start(s32[32]{0:T(128)} %param.20) | copy-start | bytes 388
  103.9 2.9 %copy-start.9 = (f32[8]{0:T(128)S(1)}, f32[8]{0:T(128)}, u32[]{:S(2)}) copy-start(f32[8]{0:T(128)} %param.17) | copy-start | bytes 100
  125.4 81.3 %copy-start.4 = (bf16[512,512]{1,0:T(8,128)(2,1)S(1)}, bf16[512,512]{1,0:T(8,128)(2,1)}, u32[]{:S(2)}) copy-start(bf16[512,512]{1,0:T(8,128)(2,1)} %param.21) | copy-start | bytes 1572868
  125.4 92.3 %copy-start.1 = (bf16[512,512]{1,0:T(8,128)(2,1)S(1)}, bf16[512,512]{1,0:T(8,128)(2,1)}, u32[]{:S(2)}) copy-start(bf16[512,512]{1,0:T(8,128)(2,1)} %param.13) | copy-start | bytes 1572868
Sparse Core Ops, SparseCore 0:
  136.3 69.1 all-reduce.3
where the time goes:
time: 225 us
  blocking collectives  86.9 us (39%)
  waiting for transfers between devices  49 us (22%)
  local copies, waits for them, and re-layouts  46.8 us (21%)
  matrix products  24.5 us (11%)
  between operations  14.3 us (6%)
  other arithmetic  2.95 us (1%)
    psum x1, waiting for transfers between devices, shards(): lax.psum((weight_sum * rescale_factor, weighted * rescale_factor[..., Non...  49 us
    slice x1, local copies, waits for them, and re-layouts, shards(): cached_keys = kv_cache[:, :, :, :head_size]  41.6 us
    psum x1, blocking collectives, shards(): lax.psum(part_query.astype(jnp.bfloat16), 'kv').astype(jnp.float32)  39.3 us
    psum x1, blocking collectives, shards(): lax.psum((weight_sum * rescale_factor, weighted * rescale_factor[..., Non...  19.6 us
    pmax x1, blocking collectives, shards(): peak = lax.pmax(peak_local, 'kv')  17.1 us
    dot_general x1, matrix products, shards(): jnp.einsum('bkgd,blkd->bkgl', query_head_rows, cached_keys, preferred_ele...  12.1 us
    psum x1, blocking collectives, shards(): mixed = lax.psum(part_out.astype(jnp.bfloat16), 'tp')  10.9 us
    dot_general x1, matrix products, shards(): jnp.einsum('bkgl,blkd->bkgd', weights.astype(jnp.bfloat16), cached_vals,...  10.7 us
  transfers between devices with their start and end apart: 1, of which 1 were waited for; matrix products, arithmetic and copies ran while one was open for 0% of the time, Pallas kernels for 0%

commit v1 on v0

--- a/solution.py
+++ b/solution.py
@@ -54,7 +54,7 @@
     part_gate = jnp.dot(normalized_input, gate_cols, preferred_element_type=jnp.float32)
     total_sq, sum_query, sum_keyval, sum_gate = (
         lax.psum(squares.astype(jnp.bfloat16), "kv").astype(jnp.float32),
-        lax.psum(part_query.astype(jnp.bfloat16), "kv").astype(jnp.float32),
+        jnp.sum(lax.all_gather(part_query.astype(jnp.bfloat16), "kv"), axis=0).astype(jnp.float32),
         lax.psum(part_keyval.astype(jnp.bfloat16), "kv").astype(jnp.float32),
         lax.psum(part_gate.astype(jnp.bfloat16), "kv").astype(jnp.float32),
     )

time: 225 us -> 256 us (1.14)
  blocking collectives: 86.9 us -> 117 us
    all_gather x0 -> x1, blocking collectives: none -> 30.7 us  [shards(): lax.all_gather(part_query.astype(jnp.bfloat16), 'kv')]
where the time goes in v1:
time: 256 us
  blocking collectives  117 us (46%)
  waiting for transfers between devices  49 us (19%)
  local copies, waits for them, and re-layouts  47 us (18%)
  matrix products  24.4 us (10%)
  between operations  14.3 us (6%)
  other arithmetic  3.73 us (1%)
    psum x1, waiting for transfers between devices, shards(): lax.psum((weight_sum * rescale_factor, weighted * rescale_factor[..., Non...  49 us
    slice x1, local copies, waits for them, and re-layouts, shards(): cached_keys = kv_cache[:, :, :, :head_size]  41.5 us
    psum x1, blocking collectives, shards(): lax.psum(squares.astype(jnp.bfloat16), 'kv').astype(jnp.float32)  38.9 us
    all_gather x1, blocking collectives, shards(): lax.all_gather(part_query.astype(jnp.bfloat16), 'kv')  30.7 us
    psum x1, blocking collectives, shards(): lax.psum((weight_sum * rescale_factor, weighted * rescale_factor[..., Non...  19.6 us
    pmax x1, blocking collectives, shards(): peak = lax.pmax(peak_local, 'kv')  17.1 us
    dot_general x1, matrix products, shards(): jnp.einsum('bkgd,blkd->bkgl', query_head_rows, cached_keys, preferred_ele...  12 us
    psum x1, blocking collectives, shards(): mixed = lax.psum(part_out.astype(jnp.bfloat16), 'tp')  10.9 us
  transfers between devices with their start and end apart: 1, of which 1 were waited for; matrix products, arithmetic and copies ran while one was open for 0% of the time, Pallas kernels for 0%

profile of v1, /device:TPU:0, one launch (start us, length us, event | category | flops | bytes accessed | tf_op | source)
XLA Modules:
  0.0 255.7 jit_solution(2277685316011079738)
XLA Ops:
  7.2 0.0 copy-start
  7.2 0.0 all-reduce.4.cloned.1.call-start
  7.2 0.7 broadcast_compare_fusion.1
  8.0 0.1 copy.40
  8.1 0.1 reshape.213
  8.2 1.8 reshape.203
  10.0 0.0 copy-start.7
  10.0 0.0 copy-start.6
  10.1 2.3 gather_fusion
  12.3 0.1 gather.7
  12.4 0.1 fusion.22
  12.6 0.1 convolution_convert_fusion.2
  12.7 0.1 convolution_convert_fusion.3
  12.9 0.8 convolution_convert_fusion.4
  13.7 0.1 copy.41
  13.8 38.9 %all-reduce.1 = (bf16[32]{0:T(256)(128)(2,1)S(1)}, bf16[32,8]{0,1:T(8,128)(2,1)S(1)}, bf16[32,256]{1,0:T(8,128)(2,1)S(1)}) all-reduce(bf16[32]{0:T(256)(128)(2,1)S(1)} %fusion.22, bf16[32,8]{0,1:T(8,128)(2,1)S(1)} %convolution_convert_fusion.4, bf16[32,256]{1,0:T(8,128)(2,1)S(1)} %pad_maximum_fusion), channel_id=1, replica_groups=mesh['kv'=8,'tp'=4] {'kv'}, use_global_device_ids=true, to_apply=%region_1.0 | all-reduce | flops 8480 | bytes 33920 | tf_op jit(solution)/shard_map/psum | solution.py:56
  52.7 0.1 multiply_convert_fusion.1
  52.7 0.1 reshape.225
  52.8 0.2 convolution_convert_fusion.1
  53.0 30.7 %all-gather = bf16[256,512]{1,0:T(8,128)(2,1)S(1)} all-gather(bf16[32,512]{1,0:T(8,128)(2,1)S(1)} %convolution_convert_fusion.1), channel_id=2, replica_groups=mesh['kv'=8,'tp'=4] {'kv'}, dimensions={0}, use_global_device_ids=true | all-gather | bytes 294912 | tf_op jit(solution)/shard_map/all_gather | solution.py:57
  83.8 0.1 reshape.209
  83.9 0.1 multiply_convert_fusion
  84.1 0.2 fusion.41
  84.3 0.1 copy.51
  84.3 0.1 broadcast_compare_fusion
  84.5 41.5 %fusion.40 = (bf16[32,1280,2,64]{3,2,1,0:T(2,128)(2,1)}, bf16[32,1280,2,64]{3,2,1,0:T(2,128)(2,1)}) fusion(bf16[32,1280,2,128]{3,2,1,0:T(2,128)(2,1)} %param.18), kind=kLoop, calls=%fused_computation.64 | loop fusion | bytes 41943040 | tf_op jit(solution)/shard_map/slice | solution.py:66
  125.9 0.0 copy-start.9
  126.0 12.0 %select_reduce_fusion = (f32[32,2,4]{2,1,0:T(2,128)S(1)}, f32[32,2,4,1280]{3,2,1,0:T(4,128)S(1)}) fusion(pred[32,1280]{1,0:T(8,128)(4,1)S(1)} %broadcast_compare_fusion, f32[32,2,4,1280]{3,2,1,0:T(4,128)S(1)} %reshape.203, bf16[32,2,4,64]{3,2,1,0:T(4,128)(2,1)S(1)} %multiply_convert_fusion, bf16[32,1280,2,64]{3,2,1,0:T(2,128)(2,1)} %get-tuple-element.14), kind=kOutput, calls=%fused_computation.8 | convolution fusion | flops 43253504 | bytes 13181952 | tf_op jit(solution)/shard_map/bkgd,blkd->bkgl/dot_general | solution.py:69
  138.0 0.1 copy.42
  138.1 0.1 broadcast_select_fusion
  138.2 0.1 copy.44
  138.3 17.1 %pmax.7 = f32[32,2,4]{0,2,1:T(4,128)S(1)} all-reduce(f32[32,2,4]{0,2,1:T(4,128)S(1)} %maximum_select_fusion), channel_id=1, replica_groups=mesh['kv'=8,'tp'=4] {'kv'}, use_global_device_ids=true, to_apply=%region_6.7 | all-reduce | flops 256 | bytes 2048 | tf_op jit(solution)/shard_map/pmax | solution.py:115
  155.4 0.8 fusion.16
  156.2 0.1 copy.48
  156.3 0.1 copy.46
  156.4 0.1 copy.47
  156.5 0.1 reshape.210
  156.6 0.0 copy-start.1
  156.6 10.7 %fusion.13 = f32[32,2,4,64]{3,2,1,0:T(4,128)} fusion(bf16[32,1280,2,64]{3,2,1,0:T(2,128)(2,1)} %get-tuple-element.15, f32[32,2,4,1280]{3,2,1,0:T(4,128)S(1)} %get-tuple-element.20, f32[32,2,4]{2,1,0:T(2,128)S(1)} %copy.44, pred[32,1280]{1,0:T(8,128)(4,1)S(1)} %broadcast_compare_fusion, f32[32,2,4]{2,1,0:T(2,128)S(1)} %copy.47, ...), kind=kOutput, calls=%fused_computation.10 | convolution fusion | flops 42975232 | bytes 11922432 | tf_op jit(solution)/shard_map/bkgl,blkd->bkgd/dot_general | solution.py:101
  167.3 0.0 all-reduce.4.cloned.1.call-update
  167.4 19.6 %all-reduce = (f32[32,2,4]{0,2,1:T(4,128)S(1)}, f32[32,2,4]{0,2,1:T(4,128)S(1)}) all-reduce(f32[32,2,4]{0,2,1:T(4,128)S(1)} %get-tuple-element.9, f32[32,2,4]{0,2,1:T(4,128)S(1)} %bitcast.33), channel_id=1, replica_groups=mesh['kv'=8,'tp'=4] {'kv'}, use_global_device_ids=true, to_apply=%region_9.10 | all-reduce | flops 512 | bytes 4096 | tf_op jit(solution)/shard_map/psum | solution.py:117
  186.9 0.6 add_add_fusion
  187.5 0.1 copy.49
  187.6 49.0 %all-reduce.4.cloned.1.call-done = f32[32,2,4,64]{3,2,1,0:T(4,128)} async-done(((f32[32,2,4,64]{3,2,1,0:T(4,128)}), f32[32,2,4,64]{3,2,1,0:T(4,128)}) %all-reduce.4.cloned.1.call-update) | async-done | bytes 65552 | tf_op jit(solution)/shard_map/psum | solution.py:117
  236.6 1.0 divide_convert_fusion
  237.7 0.1 reshape.206
  237.8 0.2 convolution_convert_fusion
  238.0 10.9 %psum.54 = bf16[32,512]{1,0:T(8,128)(2,1)} all-reduce(bf16[32,512]{1,0:T(8,128)(2,1)S(1)} %convolution_convert_fusion), channel_id=1, replica_groups=mesh['kv'=8,'tp'=4] {'tp'}, use_global_device_ids=true, to_apply=%region_10.11 | all-reduce | flops 16384 | bytes 65536 | tf_op jit(solution)/shard_map/psum | solution.py:127
  (28 shorter events, 0.2 us)
Async XLA Ops:
  7.2 45.7 %copy-start = (bf16[512,512]{1,0:T(8,128)(2,1)S(1)}, bf16[512,512]{1,0:T(8,128)(2,1)}, u32[]{:S(2)}) copy-start(bf16[512,512]{1,0:T(8,128)(2,1)} %param.13) | copy-start | bytes 1572868
  7.2 229.4 %all-reduce.4.cloned.1.call-start = ((), (), s32[]{:S(2)}) async-start(), calls=%async_computation | async-start | bytes 262144 | tf_op jit(solution)/shard_map/psum | solution.py:117
  8.2 1.8 copy-start.2
  10.0 2.4 copy-start.3
  10.0 2.5 copy-start.5
  10.0 2.5 copy-start.7
  10.0 2.7 %copy-start.6 = (bf16[512,128]{1,0:T(8,128)(2,1)S(1)}, bf16[512,128]{1,0:T(8,128)(2,1)}, u32[]{:S(2)}) copy-start(bf16[512,128]{1,0:T(8,128)(2,1)} %param.14) | copy-start | bytes 393220
  12.3 72.0 %copy-start.8 = (s32[32]{0:T(128)S(1)}, s32[32]{0:T(128)}, u32[]{:S(2)}) copy-start(s32[32]{0:T(128)} %param.20) | copy-start | bytes 388
  125.9 12.1 %copy-start.9 = (f32[8]{0:T(128)S(1)}, f32[8]{0:T(128)}, u32[]{:S(2)}) copy-start(f32[8]{0:T(128)} %param.17) | copy-start | bytes 100
  156.6 81.2 %copy-start.4 = (bf16[512,512]{1,0:T(8,128)(2,1)S(1)}, bf16[512,512]{1,0:T(8,128)(2,1)}, u32[]{:S(2)}) copy-start(bf16[512,512]{1,0:T(8,128)(2,1)} %param.21) | copy-start | bytes 1572868
  156.6 92.3 %copy-start.1 = (bf16[512,512]{1,0:T(8,128)(2,1)S(1)}, bf16[512,512]{1,0:T(8,128)(2,1)}, u32[]{:S(2)}) copy-start(bf16[512,512]{1,0:T(8,128)(2,1)} %param.13) | copy-start | bytes 1572868
Sparse Core Ops, SparseCore 0:
  167.5 69.1 all-reduce.3
